TPU v7x, 32 devices: a whole 2x2x4 slice. The times are simulated.
32 devices in a mesh: grp: 2 (over y), fs: 4 (over z), tp: 4 (over x, core).
Axes of the slice: x: 2, y: 2, z: 4, core: 2. Of those that a mesh axis runs over, the one named last changes fastest.
Arguments:
- tokens: bfloat16 [8, 1024, 2048], P(('grp', 'fs'), None, 'tp'), parts along dimension 0, may hold values from -6 to 6
- mix_gain: float32 [2048], replicated, may hold values from 0.1 to 1.9
- in_matrix: float32 [2048, 1024], P('fs', 'tp'), may hold values from -0.125 to 0.125
- in_scale: float32 [1, 1024], P(None, 'tp'), may hold values from 0.5 to 2
- pool_mix: bfloat16 [8, 128, 128], P('tp'), may hold values from -0.5 to 0.5
- pool_scale: float32 [1, 1024], P(None, 'tp'), may hold values from 0.1 to 1.9
- out_matrix: float32 [1024, 2048], P('tp', 'fs'), may hold values from -0.25 to 0.25
- out_scale: float32 [1, 2048], P(None, 'fs'), may hold values from 0.5 to 2
- ffn_gain: float32 [2048], replicated, may hold values from 0.1 to 1.9
- gate_matrix: float32 [2048, 5632], P('fs', 'tp'), may hold values from -0.125 to 0.125
- gate_scale: float32 [1, 5632], P(None, 'tp'), may hold values from 0.5 to 2
- up_matrix: float32 [2048, 5632], P('fs', 'tp'), may hold values from -0.125 to 0.125
- up_scale: float32 [1, 5632], P(None, 'tp'), may hold values from 0.5 to 2
- gate_taps: float32 [3, 5632], P(None, 'tp'), may hold values from -4 to 4
- up_taps: float32 [3, 5632], P(None, 'tp'), may hold values from -4 to 4
- down_matrix: float32 [5632, 2048], P('tp', 'fs'), may hold values from -0.109375 to 0.109375
- down_scale: float32 [1, 2048], P(None, 'fs'), may hold values from 0.5 to 2
Outputs:
- layer_out: bfloat16 [8, 1024, 2048], P(('grp', 'fs'), None, 'tp'), parts along dimension 0
There are 2 independent parts, one for each index of `grp`. A program takes and returns all parts, laid end to end along the dimension named above; an argument that names none is the same for every part. Nothing has to cross between parts.
All inputs are finite; a program needn't handle non-finite values.
Results may differ from a plain program's by a relative error of at most 0.025.
Values may be sent and summed in bfloat16 or wider, within the bound.
No kernel may reach another device: no remote copies, remote signals or barrier semaphores. Data moves between devices by JAX's collectives and lax.ppermute only.
A program may use at most 128 MiB of HBM per device.

v0:
```python
import jax
import jax.numpy as jnp
from jax import lax
from jax.sharding import PartitionSpec as P

BLOCKS = 8
eps = 1e-06
widest_span = 16


def norm_rows(tok_rows, norm_gain):
    values = tok_rows.astype(jnp.float32)
    scaled = values * lax.rsqrt(jnp.mean(values * values, axis=-1, keepdims=True) + eps)
    return (scaled * norm_gain).astype(jnp.bfloat16)


def span_widths(block_ids):
    return jnp.left_shift(jnp.ones_like(block_ids), 1 + 4 * block_ids // BLOCKS)


def trailing_gap(projected, windows):
    values = projected.astype(jnp.float32)
    length = values.shape[0]
    running = values
    for offset in range(1, widest_span):
        shifted = jnp.pad(values[: length - offset], ((offset, 0), (0, 0)))
        running = running + jnp.where(windows[None, :] > offset, shifted, jnp.zeros_like(shifted))
    positions = jnp.arange(length, dtype=jnp.int32)[:, None]
    counts = jnp.minimum(positions + 1, windows[None, :]).astype(jnp.float32)
    return (running / counts - values).astype(jnp.bfloat16)


def causal_taps(linear, tap_table):
    values = linear.astype(jnp.float32)
    length = values.shape[0]
    back_one = jnp.pad(values[: length - 1], ((1, 0), (0, 0)))
    back_two = jnp.pad(values[: length - 2], ((2, 0), (0, 0)))
    return tap_table[2] * values + tap_table[1] * back_one + tap_table[0] * back_two


def fold_rows(operand, portion):
    return jnp.dot(operand, portion, preferred_element_type=jnp.float32)


def shards(
    tokens,
    mix_gain,
    in_matrix,
    in_scale,
    pool_mix,
    pool_scale,
    out_matrix,
    out_scale,
    ffn_gain,
    gate_matrix,
    gate_scale,
    up_matrix,
    up_scale,
    gate_taps,
    up_taps,
    down_matrix,
    down_scale,
):
    length = tokens.shape[1]
    own_width = tokens.shape[2]
    local_rows = tokens.reshape(length, own_width)
    gathered = lax.all_gather(local_rows, "tp", axis=1, tiled=True)
    normed = norm_rows(gathered, mix_gain)
    width_in = in_matrix.shape[1]
    in_total = fold_rows(
        normed, lax.all_gather(in_matrix.astype(jnp.bfloat16), "fs", axis=0, tiled=True)
    )
    projected = (in_total * in_scale).astype(jnp.bfloat16)
    local_blocks = pool_mix.shape[0]
    block_width = pool_mix.shape[1]
    block_ids = lax.axis_index("tp") * local_blocks + jnp.arange(local_blocks, dtype=jnp.int32)
    windows = jnp.repeat(span_widths(block_ids), block_width)
    spread = trailing_gap(projected, windows)
    block_mixed = jnp.einsum(
        "lbc,bce->lbe",
        spread.reshape(length, local_blocks, block_width),
        pool_mix,
        preferred_element_type=jnp.float32,
    ).reshape(length, width_in)
    pooled = (block_mixed * pool_scale).astype(jnp.bfloat16)
    out_cols = lax.all_gather(out_scale, "fs", axis=1, tiled=True)
    tp_index = lax.axis_index("tp")
    groups = lax.axis_size("tp")
    pooled_all = lax.all_gather(pooled, "tp", axis=1, tiled=True)
    row_block = lax.all_gather(out_matrix.astype(jnp.bfloat16), "fs", axis=1, tiled=True)
    own_matrix = lax.all_to_all(row_block, "tp", split_axis=1, concat_axis=0, tiled=True)
    own_scales = lax.dynamic_slice_in_dim(out_cols, tp_index * own_width, own_width, 1)
    grouped_rows = pooled_all.reshape(length, groups, width_in)
    grouped_matrix = own_matrix.reshape(groups, width_in, own_width)
    pieces = (
        jnp.einsum("lgc,gcd->gld", grouped_rows, grouped_matrix, preferred_element_type=jnp.float32)
        * own_scales[None]
    )
    rounded = lax.optimization_barrier(pieces.astype(jnp.bfloat16))
    mixing = jnp.sum(rounded.astype(jnp.float32), axis=0)
    residual = (local_rows.astype(jnp.float32) + mixing).astype(jnp.bfloat16)
    gathered_ffn = lax.all_gather(residual, "tp", axis=1, tiled=True)
    normed_ffn = norm_rows(gathered_ffn, ffn_gain)
    gate_cast = gate_matrix.astype(jnp.bfloat16)
    up_cast = up_matrix.astype(jnp.bfloat16)
    gate_full, up_full = (
        lax.all_gather(gate_cast, "fs", axis=0, tiled=True),
        lax.all_gather(up_cast, "fs", axis=0, tiled=True),
    )
    gate_total = jnp.dot(normed_ffn, gate_full, preferred_element_type=jnp.float32)
    up_total = jnp.dot(normed_ffn, up_full, preferred_element_type=jnp.float32)
    gate_lin = (gate_total * gate_scale).astype(jnp.bfloat16)
    up_lin = (up_total * up_scale).astype(jnp.bfloat16)
    hidden = (jax.nn.silu(causal_taps(gate_lin, gate_taps)) * causal_taps(up_lin, up_taps)).astype(
        jnp.bfloat16
    )
    down_cols = lax.all_gather(down_scale, "fs", axis=1, tiled=True)
    partial_ffn = (
        jnp.dot(
            hidden,
            lax.all_gather(down_matrix.astype(jnp.bfloat16), "fs", axis=1, tiled=True),
            preferred_element_type=jnp.float32,
        )
        * down_cols
    )
    feed_out = lax.psum_scatter(
        partial_ffn.astype(jnp.bfloat16), "tp", scatter_dimension=1, tiled=True
    ).astype(jnp.float32)
    result = (residual.astype(jnp.float32) + feed_out).astype(jnp.bfloat16)
    return result.reshape(1, length, result.shape[1])


def solution(mesh):
    return jax.shard_map(
        shards,
        mesh=mesh,
        in_specs=(
            P(("grp", "fs"), None, "tp"),
            P(),
            P("fs", "tp"),
            P(None, "tp"),
            P("tp", None, None),
            P(None, "tp"),
            P("tp", "fs"),
            P(None, "fs"),
            P(),
            P("fs", "tp"),
            P(None, "tp"),
            P("fs", "tp"),
            P(None, "tp"),
            P(None, "tp"),
            P(None, "tp"),
            P("tp", "fs"),
            P(None, "fs"),
        ),
        out_specs=P(("grp", "fs"), None, "tp"),
        check_vma=False,
    )
```

profile of v0, /device:TPU:0, one launch (start us, length us, event | category | flops | bytes accessed | tf_op | source)
XLA Modules:
  0.0 573.4 jit_solution(17679194408588764987)
XLA Ops:
  11.3 34.8 %all-gather.24.cloned.1.call-done = bf16[1,1024,2048]{2,1,0:T(8,128)(2,1)} async-done(((bf16[1,1024,512]{2,1,0:T(8,128)(2,1)}), bf16[1,1024,2048]{2,1,0:T(8,128)(2,1)}) %all-gather.24.cloned.1.call-update) | async-done | bytes 4194320 | tf_op jit(solution)/shard_map/all_gather | solution.py:67
  46.1 3.1 fusion.3
  49.2 26.5 %all-gather.10.cloned.1.call-done = bf16[2048,256]{1,0:T(8,128)(2,1)} async-done(((bf16[512,256]{1,0:T(8,128)(2,1)}), bf16[2048,256]{1,0:T(8,128)(2,1)}) %all-gather.10.cloned.1.call-update) | async-done | bytes 1048592 | tf_op jit(solution)/shard_map/all_gather | solution.py:71
  75.7 3.8 fusion.20
  80.1 3.2 fusion.28
  84.3 20.3 %all-gather.14.cloned.1.call-done = bf16[256,2048]{0,1:T(8,128)(2,1)} async-done(((bf16[256,512]{0,1:T(8,128)(2,1)}), bf16[256,2048]{0,1:T(8,128)(2,1)}) %all-gather.14.cloned.1.call-update) | async-done | bytes 1048592 | tf_op jit(solution)/shard_map/all_gather | solution.py:90
  104.7 2.3 copy.23
  106.9 3.5 all-to-all-start
  110.5 11.9 %all_gather.34 = f32[1,2048]{1,0:T(1,128)S(1)} all-gather(f32[1,512]{1,0:T(1,128)S(1)} %copy-done.10), channel_id=1, replica_groups=mesh['grp'=2,'fs'=4,'tp'=4] {'fs'}, dimensions={1}, use_global_device_ids=true | all-gather | bytes 10240 | tf_op jit(solution)/shard_map/all_gather | solution.py:86
  122.5 12.5 %all-to-all-done = bf16[256,4,512]{2,0,1:T(8,128)(2,1)S(1)} async-done(((bf16[256,4,512]{2,0,1:T(8,128)(2,1)}), bf16[256,4,512]{2,0,1:T(8,128)(2,1)S(1)}, u32[]{:S(2)}, u32[]{:S(2)}) %all-to-all-start) | async-done | bytes 1048608 | tf_op jit(solution)/shard_map/all_to_all | solution.py:91
  135.0 2.7 all-gather.12.cloned.1.call-done
  137.6 3.0 multiply_convert_fusion.1
  144.2 3.3 convert_element_type.136
  149.0 12.1 %all_gather.39 = f32[1,2048]{1,0:T(1,128)S(1)} all-gather(f32[1,512]{1,0:T(1,128)S(1)} %copy-done.11), channel_id=1, replica_groups=mesh['grp'=2,'fs'=4,'tp'=4] {'fs'}, dimensions={1}, use_global_device_ids=true | all-gather | bytes 10240 | tf_op jit(solution)/shard_map/all_gather | solution.py:117
  161.2 14.5 %all-gather.16.cloned.1.call-done = bf16[1024,2048]{1,0:T(8,128)(2,1)} async-done(((bf16[1024,512]{1,0:T(8,128)(2,1)}), bf16[1024,2048]{1,0:T(8,128)(2,1)}) %all-gather.16.cloned.1.call-update) | async-done | bytes 4194320 | tf_op jit(solution)/shard_map/all_gather | solution.py:102
  175.7 3.1 fusion
  178.8 105.1 %all-gather.18.cloned.1.call-done = bf16[2048,1408]{1,0:T(8,128)(2,1)} async-done(((bf16[512,1408]{1,0:T(8,128)(2,1)}), bf16[2048,1408]{1,0:T(8,128)(2,1)}) %all-gather.18.cloned.1.call-update) | async-done | bytes 5767184 | tf_op jit(solution)/shard_map/all_gather | solution.py:107
  283.9 11.9 %fusion.11 = f32[1024,1408]{1,0:T(8,128)} fusion(bf16[2048,1408]{1,0:T(8,128)(2,1)} %all-gather.18.cloned.1.call-done, f32[1408]{0:T(1024)S(1)} %reduce.1, bf16[1024,2048]{1,0:T(8,128)(2,1)} %all-gather.16.cloned.1.call-done, f32[2048]{0:T(1024)S(1)} %copy-done.14, f32[1024]{0:T(1024)S(1)} %add_rsqrt_fusion), kind=kOutput, calls=%fused_computation.20 | convolution fusion | flops 5918294016 | bytes 15746560 | tf_op jit(solution)/shard_map/dot_general | solution.py:110
  295.8 94.7 %all-gather.20.cloned.1.call-done = bf16[2048,1408]{1,0:T(8,128)(2,1)} async-done(((bf16[512,1408]{1,0:T(8,128)(2,1)}), bf16[2048,1408]{1,0:T(8,128)(2,1)}) %all-gather.20.cloned.1.call-update) | async-done | bytes 5767184 | tf_op jit(solution)/shard_map/all_gather | solution.py:108
  390.4 12.0 %fusion.12 = f32[1024,1408]{1,0:T(8,128)} fusion(bf16[2048,1408]{1,0:T(8,128)(2,1)} %all-gather.20.cloned.1.call-done, f32[1408]{0:T(1024)S(1)} %reduce.5, bf16[1024,2048]{1,0:T(8,128)(2,1)} %all-gather.16.cloned.1.call-done, f32[2048]{0:T(1024)S(1)} %copy-done.14, f32[1024]{0:T(1024)S(1)} %add_rsqrt_fusion), kind=kOutput, calls=%fused_computation.21 | convolution fusion | flops 5918294016 | bytes 15746560 | tf_op jit(solution)/shard_map/dot_general | solution.py:111
  402.4 94.6 %all-gather.22.cloned.1.call-done = bf16[1408,2048]{1,0:T(8,128)(2,1)} async-done(((bf16[1408,512]{1,0:T(8,128)(2,1)}), bf16[1408,2048]{1,0:T(8,128)(2,1)}) %all-gather.22.cloned.1.call-update) | async-done | bytes 5767184 | tf_op jit(solution)/shard_map/all_gather | solution.py:121
  497.0 24.6 %multiply_convert_fusion = bf16[1024,2048]{1,0:T(8,128)(2,1)} fusion(bf16[1408,2048]{1,0:T(8,128)(2,1)} %all-gather.22.cloned.1.call-done, f32[2048]{0:T(1024)S(1)} %bitcast.83, f32[1022,1408]{1,0:T(8,128)} %bitcast.89, f32[1023,1408]{1,0:T(8,128)} %bitcast.90, f32[1024,1408]{1,0:T(8,128)} %fusion.12, f32[1022,1408]{1,0:T(8,128)} %bitcast.87, ...), kind=kOutput, calls=%fused_computation.10 | convolution fusion | flops 5932843008 | bytes 44572672 | tf_op jit(solution)/shard_map/dot_general | solution.py:119
  521.6 42.8 %reduce-scatter.2.cloned.1.call-done = bf16[1024,512]{1,0:T(8,128)(2,1)} async-done(((bf16[1024,2048]{1,0:T(8,128)(2,1)}), bf16[1024,512]{1,0:T(8,128)(2,1)}) %reduce-scatter.2.cloned.1.call-update) | async-done | bytes 1048592 | tf_op jit(solution)/shard_map/reduce_scatter | solution.py:126
  564.4 2.5 fusion.25
  (75 shorter events, 11.3 us)
Async XLA Ops:
  6.5 73.6 %copy-start = (bf16[2,128,128]{2,1,0:T(8,128)(2,1)S(1)}, bf16[2,128,128]{2,1,0:T(8,128)(2,1)}, u32[]{:S(2)}) copy-start(bf16[2,128,128]{2,1,0:T(8,128)(2,1)} %param.21) | copy-start | bytes 196612
  6.5 69.2 %copy-start.15 = (f32[1,256]{1,0:T(1,128)S(1)}, f32[1,256]{1,0:T(1,128)}, u32[]{:S(2)}) copy-start(f32[1,256]{1,0:T(1,128)} %param.20) | copy-start | bytes 3076
  6.5 69.2 %copy-start.13 = (f32[2048]{0:T(1024)S(1)}, f32[2048]{0:T(1024)}, u32[]{:S(2)}) copy-start(f32[2048]{0:T(1024)} %param.18) | copy-start | bytes 24580
  6.5 39.6 %all-gather.24.cloned.1.call-start = ((), (), s32[]{:S(2)}) async-start(), calls=%async_computation.10 | async-start | bytes 5242880 | tf_op jit(solution)/shard_map/all_gather | solution.py:67
  7.3 68.4 %all-gather.10.cloned.1.call-start = ((), (), s32[]{:S(2)}) async-start(), calls=%async_computation.2 | async-start | bytes 1310720 | tf_op jit(solution)/shard_map/all_gather | solution.py:71
  9.1 95.6 %all-gather.14.cloned.1.call-start = ((), (), s32[]{:S(2)}) async-start(), calls=%async_computation.4 | async-start | bytes 1310720 | tf_op jit(solution)/shard_map/all_gather | solution.py:90
  11.1 126.6 %all-gather.12.cloned.1.call-start = ((), (), s32[]{:S(2)}) async-start(), calls=%async_computation.3 | async-start | bytes 2621440 | tf_op jit(solution)/shard_map/all_gather | solution.py:89
  83.4 27.1 %copy-start.10 = (f32[1,512]{1,0:T(1,128)S(1)}, f32[1,512]{1,0:T(1,128)}, u32[]{:S(2)}) copy-start(f32[1,512]{1,0:T(1,128)} %param.24) | copy-start | bytes 6148
  106.9 28.0 %all-to-all-start = ((bf16[256,4,512]{2,0,1:T(8,128)(2,1)}), bf16[256,4,512]{2,0,1:T(8,128)(2,1)S(1)}, u32[]{:S(2)}, u32[]{:S(2)}) async-start(bf16[256,4,512]{2,0,1:T(8,128)(2,1)} %copy.23), calls=%async_computation | async-start | bytes 2097152 | tf_op jit(solution)/shard_map/all_to_all | solution.py:91
  110.5 65.3 %all-gather.16.cloned.1.call-start = ((), (), s32[]{:S(2)}) async-start(), calls=%async_computation.5 | async-start | bytes 5242880 | tf_op jit(solution)/shard_map/all_gather | solution.py:102
  137.6 3.7 copy-start.3
  142.7 141.2 %all-gather.18.cloned.1.call-start = ((), (), s32[]{:S(2)}) async-start(), calls=%async_computation.6 | async-start | bytes 7208960 | tf_op jit(solution)/shard_map/all_gather | solution.py:107
  144.0 3.5 copy-start.5
  144.1 4.8 copy-start.8
  144.1 4.9 copy-start.9
  144.1 4.9 copy-start.11
  144.1 17.0 %copy-start.6 = (f32[3,1408]{1,0:T(4,128)S(1)}, f32[3,1408]{1,0:T(4,128)}, u32[]{:S(2)}) copy-start(f32[3,1408]{1,0:T(4,128)} %param.31) | copy-start | bytes 50692
  144.1 17.0 %copy-start.7 = (f32[3,1408]{1,0:T(4,128)S(1)}, f32[3,1408]{1,0:T(4,128)}, u32[]{:S(2)}) copy-start(f32[3,1408]{1,0:T(4,128)} %param.30) | copy-start | bytes 50692
  144.1 246.3 %all-gather.20.cloned.1.call-start = ((), (), s32[]{:S(2)}) async-start(), calls=%async_computation.7 | async-start | bytes 7208960 | tf_op jit(solution)/shard_map/all_gather | solution.py:108
  147.5 136.4 %copy-start.14 = (f32[2048]{0:T(1024)S(1)}, f32[2048]{0:T(1024)}, u32[]{:S(2)}) copy-start(f32[2048]{0:T(1024)} %param.25) | copy-start | bytes 24580
  147.5 349.5 %all-gather.22.cloned.1.call-start = ((), (), s32[]{:S(2)}) async-start(), calls=%async_computation.8 | async-start | bytes 7208960 | tf_op jit(solution)/shard_map/all_gather | solution.py:121
  148.8 415.6 %reduce-scatter.2.cloned.1.call-start = ((), (), s32[]{:S(2)}) async-start(), calls=%async_computation.9 | async-start | bytes 5242880 | tf_op jit(solution)/shard_map/reduce_scatter | solution.py:126
  497.0 67.4 %copy-start.2 = (bf16[1024,512]{1,0:T(8,128)(2,1)S(1)}, bf16[1024,512]{1,0:T(8,128)(2,1)}, u32[]{:S(2)}) copy-start(bf16[1024,512]{1,0:T(8,128)(2,1)} %fusion.13) | copy-start | bytes 3145732
  497.0 69.9 %copy-start.1 = (bf16[2,128,128]{2,1,0:T(8,128)(2,1)S(1)}, bf16[2,128,128]{2,1,0:T(8,128)(2,1)}, u32[]{:S(2)}) copy-start(bf16[2,128,128]{2,1,0:T(8,128)(2,1)} %param.21) | copy-start | bytes 196612
  (2 other events, 5.4 us)
Sparse Core Ops, SparseCore 0:
  8.9 37.1 all-gather.23
  47.7 27.9 all-gather.9
  77.3 27.3 all-gather.13
  106.1 31.4 all-gather.11
  142.8 32.9 all-gather.15
  177.2 106.6 all-gather.17
  285.5 104.9 all-gather.19
  392.0 104.9 all-gather.21
  521.8 42.6 reduce-scatter.1
where the time goes:
time: 574 us; the launch traced here: 573 us
  waiting for transfers between devices  449 us (78%)
  matrix products  58.5 us (10%)
  blocking collectives  24.1 us (4%)
  other arithmetic  19.3 us (3%)
  between operations  13.5 us (2%)
    all_gather x1, waiting for transfers between devices, shards(): lax.all_gather(gate_cast, 'fs', axis=0, tiled=True)  105 us
    all_gather x1, waiting for transfers between devices, shards(): lax.all_gather(up_cast, 'fs', axis=0, tiled=True)  94.7 us
    all_gather x1, waiting for transfers between devices, shards(): lax.all_gather(down_matrix.astype(jnp.bfloat16), 'fs', axis=1, tiled=True)  94.6 us
    reduce_scatter x1, waiting for transfers between devices, shards(): lax.psum_scatter(partial_ffn.astype(jnp.bfloat16), 'tp', scatter_dimensio...  42.8 us
    all_gather x1, waiting for transfers between devices, shards(): gathered = lax.all_gather(local_rows, 'tp', axis=1, tiled=True)  34.8 us
    all_gather x1, waiting for transfers between devices, shards(): lax.all_gather(in_matrix.astype(jnp.bfloat16), 'fs', axis=0, tiled=True)  26.5 us
    dot_general x1, matrix products, shards(): jnp.dot(hidden, lax.all_gather(down_matrix.astype(jnp.bfloat16), 'fs', ax...  24.6 us
    all_gather x1, waiting for transfers between devices, shards(): lax.all_gather(out_matrix.astype(jnp.bfloat16), 'fs', axis=1, tiled=True)  20.3 us
  transfers between devices with their start and end apart: 10, of which 10 were waited for; matrix products, arithmetic and copies ran while one was open for 9% of the time, Pallas kernels for 0%

commit v1 on v0

--- a/solution.py
+++ b/solution.py
@@ -1,3 +1,4 @@
+import functools
 import jax
 import jax.numpy as jnp
 from jax import lax
@@ -6,6 +7,22 @@
 BLOCKS = 8
 eps = 1e-06
 widest_span = 16
+
+
+def _press_weights(obj, shard_axis):
+    now, side_arr = (jax.lax.axis_size(shard_axis), jax.lax.axis_index(shard_axis))
+    e_next, left_arr = (obj, 1)
+    while left_arr < now:
+        frame_out = tuple(((hop_no, hop_no ^ left_arr) for hop_no in range(now)))
+        block_next = jax.lax.ppermute(e_next, shard_axis, frame_out)
+        w1 = jnp.concatenate([e_next, block_next], axis=1)
+        y1 = jnp.concatenate([block_next, e_next], axis=1)
+        e_next = jnp.where(side_arr & left_arr == 0, w1, y1)
+        left_arr = 2 * left_arr
+    return e_next
+
+
+pair_orders_for = functools.partial(_press_weights, shard_axis="fs")
 
 
 def norm_rows(tok_rows, norm_gain):
@@ -118,7 +135,7 @@
     partial_ffn = (
         jnp.dot(
             hidden,
-            lax.all_gather(down_matrix.astype(jnp.bfloat16), "fs", axis=1, tiled=True),
+            pair_orders_for(down_matrix.astype(jnp.bfloat16)),
             preferred_element_type=jnp.float32,
         )
         * down_cols

time: 574 us -> 594 us (1.035)
  blocking collectives: 24.1 us -> 51.5 us
  waiting for transfers between devices: 449 us -> 432 us
    all_gather x1 -> x0, waiting for transfers between devices: 94.6 us -> none  [shards(): lax.all_gather(down_matrix.astype(jnp.bfloat16), 'fs', axis=1, tiled=True)]
    all_gather x1, waiting for transfers between devices: 105 us -> 194 us  [shards(): lax.all_gather(gate_cast, 'fs', axis=0, tiled=True)]
    all_gather x1, blocking collectives: 12.1 us -> 39.5 us  [shards(): down_cols = lax.all_gather(down_scale, 'fs', axis=1, tiled=True)]
    all_gather x1, waiting for transfers between devices: 14.5 us -> 0.01 us  [shards(): gathered_ffn = lax.all_gather(residual, 'tp', axis=1, tiled=True)]
  transfers between devices with their start and end apart: 10 -> 11, of which waited for: 10 -> 8; matrix products, arithmetic and copies ran while one was open for 9% -> 9% of each run, Pallas kernels for 0% -> 0%
where the time goes in v1:
time: 594 us; the launch traced here: 593 us
  waiting for transfers between devices  432 us (73%)
  matrix products  61.4 us (10%)
  blocking collectives  51.5 us (9%)
  other arithmetic  22.3 us (4%)
  between operations  13.8 us (2%)
  local copies, waits for them, and re-layouts  6.49 us (1%)
  starting transfers between devices  6.19 us (1%)
    all_gather x1, waiting for transfers between devices, shards(): lax.all_gather(gate_cast, 'fs', axis=0, tiled=True)  194 us
    all_gather x1, waiting for transfers between devices, shards(): lax.all_gather(up_cast, 'fs', axis=0, tiled=True)  97.5 us
    reduce_scatter x1, waiting for transfers between devices, shards(): lax.psum_scatter(partial_ffn.astype(jnp.bfloat16), 'tp', scatter_dimensio...  42.7 us
    all_gather x1, blocking collectives, shards(): down_cols = lax.all_gather(down_scale, 'fs', axis=1, tiled=True)  39.5 us
    all_gather x1, waiting for transfers between devices, shards(): gathered = lax.all_gather(local_rows, 'tp', axis=1, tiled=True)  34.8 us
    dot_general x1, matrix products, shards(): jnp.dot(hidden, pair_orders_for(down_matrix.astype(jnp.bfloat16)), prefer...  27.6 us
    all_gather x1, waiting for transfers between devices, shards(): lax.all_gather(in_matrix.astype(jnp.bfloat16), 'fs', axis=0, tiled=True)  26.5 us
    all_gather x1, waiting for transfers between devices, shards(): lax.all_gather(out_matrix.astype(jnp.bfloat16), 'fs', axis=1, tiled=True)  20.3 us
  transfers between devices with their start and end apart: 11, of which 8 were waited for; matrix products, arithmetic and copies ran while one was open for 9% of the time, Pallas kernels for 0%

profile of v1, /device:TPU:0, one launch (start us, length us, event | category | flops | bytes accessed | tf_op | source)
XLA Modules:
  0.0 593.3 jit_solution(5893123763095650738)
XLA Ops:
  11.3 34.8 %all-gather.21.cloned.1.call-done = bf16[1,1024,2048]{2,1,0:T(8,128)(2,1)} async-done(((bf16[1,1024,512]{2,1,0:T(8,128)(2,1)}), bf16[1,1024,2048]{2,1,0:T(8,128)(2,1)}) %all-gather.21.cloned.1.call-update) | async-done | bytes 4194320 | tf_op jit(solution)/shard_map/all_gather | solution.py:84
  46.1 3.1 fusion.3
  49.2 26.5 %all-gather.9.cloned.1.call-done = bf16[2048,256]{1,0:T(8,128)(2,1)} async-done(((bf16[512,256]{1,0:T(8,128)(2,1)}), bf16[2048,256]{1,0:T(8,128)(2,1)}) %all-gather.9.cloned.1.call-update) | async-done | bytes 1048592 | tf_op jit(solution)/shard_map/all_gather | solution.py:88
  75.7 3.8 fusion.27
  80.1 3.2 fusion.35
  84.3 20.3 %all-gather.13.cloned.1.call-done = bf16[256,2048]{0,1:T(8,128)(2,1)} async-done(((bf16[256,512]{0,1:T(8,128)(2,1)}), bf16[256,2048]{0,1:T(8,128)(2,1)}) %all-gather.13.cloned.1.call-update) | async-done | bytes 1048592 | tf_op jit(solution)/shard_map/all_gather | solution.py:107
  104.7 2.3 copy.23
  106.9 3.5 all-to-all-start
  110.5 11.9 %all_gather.31 = f32[1,2048]{1,0:T(1,128)S(1)} all-gather(f32[1,512]{1,0:T(1,128)S(1)} %copy-done.9), channel_id=1, replica_groups=mesh['grp'=2,'fs'=4,'tp'=4] {'fs'}, dimensions={1}, use_global_device_ids=true | all-gather | bytes 10240 | tf_op jit(solution)/shard_map/all_gather | solution.py:103
  122.5 12.5 %all-to-all-done = bf16[256,4,512]{2,0,1:T(8,128)(2,1)S(1)} async-done(((bf16[256,4,512]{2,0,1:T(8,128)(2,1)}), bf16[256,4,512]{2,0,1:T(8,128)(2,1)S(1)}, u32[]{:S(2)}, u32[]{:S(2)}) %all-to-all-start) | async-done | bytes 1048608 | tf_op jit(solution)/shard_map/all_to_all | solution.py:108
  135.0 2.7 all-gather.11.cloned.1.call-done
  137.6 3.0 multiply_convert_fusion.1
  144.1 3.2 convert_element_type.136
  147.3 2.3 convert_element_type.140
  151.2 39.5 %all_gather.35 = f32[1,2048]{1,0:T(1,128)S(1)} all-gather(f32[1,512]{1,0:T(1,128)S(1)} %copy-done.10), channel_id=1, replica_groups=mesh['grp'=2,'fs'=4,'tp'=4] {'fs'}, dimensions={1}, use_global_device_ids=true | all-gather | bytes 10240 | tf_op jit(solution)/shard_map/all_gather | solution.py:134
  190.9 2.0 maximum_select_fusion.4
  193.8 3.1 fusion
  196.9 193.8 %all-gather.17.cloned.1.call-done = bf16[2048,1408]{1,0:T(8,128)(2,1)} async-done(((bf16[512,1408]{1,0:T(8,128)(2,1)}), bf16[2048,1408]{1,0:T(8,128)(2,1)}) %all-gather.17.cloned.1.call-update) | async-done | bytes 5767184 | tf_op jit(solution)/shard_map/all_gather | solution.py:124
  390.8 12.0 %fusion.18 = f32[1024,1408]{1,0:T(8,128)} fusion(bf16[2048,1408]{1,0:T(8,128)(2,1)} %all-gather.17.cloned.1.call-done, f32[1408]{0:T(1024)S(1)} %reduce.1, bf16[1024,2048]{1,0:T(8,128)(2,1)} %all-gather.15.cloned.1.call-done, f32[2048]{0:T(1024)S(1)} %copy-done.14, f32[1024]{0:T(1024)S(1)} %add_rsqrt_fusion), kind=kOutput, calls=%fused_computation.28 | convolution fusion | flops 5918294016 | bytes 15746560 | tf_op jit(solution)/shard_map/dot_general | solution.py:127
  402.8 97.5 %all-gather.19.cloned.1.call-done = bf16[2048,1408]{1,0:T(8,128)(2,1)} async-done(((bf16[512,1408]{1,0:T(8,128)(2,1)}), bf16[2048,1408]{1,0:T(8,128)(2,1)}) %all-gather.19.cloned.1.call-update) | async-done | bytes 5767184 | tf_op jit(solution)/shard_map/all_gather | solution.py:125
  500.2 11.9 %fusion.19 = f32[1024,1408]{1,0:T(8,128)} fusion(bf16[2048,1408]{1,0:T(8,128)(2,1)} %all-gather.19.cloned.1.call-done, f32[1408]{0:T(1024)S(1)} %reduce.5, bf16[1024,2048]{1,0:T(8,128)(2,1)} %all-gather.15.cloned.1.call-done, f32[2048]{0:T(1024)S(1)} %copy-done.14, f32[1024]{0:T(1024)S(1)} %add_rsqrt_fusion), kind=kOutput, calls=%fused_computation.29 | convolution fusion | flops 5918294016 | bytes 15746560 | tf_op jit(solution)/shard_map/dot_general | solution.py:128
  513.7 27.6 %multiply_convert_fusion = bf16[1024,2048]{1,0:T(8,128)(2,1)} fusion(f32[2048]{0:T(1024)S(1)} %bitcast.82, bf16[1408,1024]{1,0:T(8,128)(2,1)} %copy-done.12, bf16[1408,1024]{1,0:T(8,128)(2,1)} %maximum_select_fusion.4, pred[]{:T(512)S(6)} %eq.6, f32[1022,1408]{1,0:T(8,128)} %bitcast.88, f32[1023,1408]{1,0:T(8,128)} %bitcast.89, f32[1024,1408]{1,0:T(8,128)} %fusion.19, ...), kind=kOutput, calls=%fused_computation.10 | convolution fusion | flops 5958795264 | bytes 44572672 | tf_op jit(solution)/shard_map/dot_general | solution.py:136
  541.2 42.7 %reduce-scatter.2.cloned.1.call-done = bf16[1024,512]{1,0:T(8,128)(2,1)} async-done(((bf16[1024,2048]{1,0:T(8,128)(2,1)}), bf16[1024,512]{1,0:T(8,128)(2,1)}) %reduce-scatter.2.cloned.1.call-update) | async-done | bytes 1048592 | tf_op jit(solution)/shard_map/reduce_scatter | solution.py:143
  583.9 2.5 fusion.32
  (77 shorter events, 13.9 us)
Async XLA Ops:
  6.5 73.6 %copy-start = (bf16[2,128,128]{2,1,0:T(8,128)(2,1)S(1)}, bf16[2,128,128]{2,1,0:T(8,128)(2,1)}, u32[]{:S(2)}) copy-start(bf16[2,128,128]{2,1,0:T(8,128)(2,1)} %param.21) | copy-start | bytes 196612
  6.5 69.2 %copy-start.15 = (f32[1,256]{1,0:T(1,128)S(1)}, f32[1,256]{1,0:T(1,128)}, u32[]{:S(2)}) copy-start(f32[1,256]{1,0:T(1,128)} %param.20) | copy-start | bytes 3076
  6.5 69.2 %copy-start.13 = (f32[2048]{0:T(1024)S(1)}, f32[2048]{0:T(1024)}, u32[]{:S(2)}) copy-start(f32[2048]{0:T(1024)} %param.18) | copy-start | bytes 24580
  6.5 39.6 %all-gather.21.cloned.1.call-start = ((), (), s32[]{:S(2)}) async-start(), calls=%async_computation.9 | async-start | bytes 5242880 | tf_op jit(solution)/shard_map/all_gather | solution.py:84
  7.3 68.4 %all-gather.9.cloned.1.call-start = ((), (), s32[]{:S(2)}) async-start(), calls=%async_computation.2 | async-start | bytes 1310720 | tf_op jit(solution)/shard_map/all_gather | solution.py:88
  9.1 95.6 %all-gather.13.cloned.1.call-start = ((), (), s32[]{:S(2)}) async-start(), calls=%async_computation.4 | async-start | bytes 1310720 | tf_op jit(solution)/shard_map/all_gather | solution.py:107
  11.1 126.6 %all-gather.11.cloned.1.call-start = ((), (), s32[]{:S(2)}) async-start(), calls=%async_computation.3 | async-start | bytes 2621440 | tf_op jit(solution)/shard_map/all_gather | solution.py:106
  83.4 27.1 %copy-start.9 = (f32[1,512]{1,0:T(1,128)S(1)}, f32[1,512]{1,0:T(1,128)}, u32[]{:S(2)}) copy-start(f32[1,512]{1,0:T(1,128)} %param.24) | copy-start | bytes 6148
  106.9 28.0 %all-to-all-start = ((bf16[256,4,512]{2,0,1:T(8,128)(2,1)}), bf16[256,4,512]{2,0,1:T(8,128)(2,1)S(1)}, u32[]{:S(2)}, u32[]{:S(2)}) async-start(bf16[256,4,512]{2,0,1:T(8,128)(2,1)} %copy.23), calls=%async_computation | async-start | bytes 2097152 | tf_op jit(solution)/shard_map/all_to_all | solution.py:108
  110.5 83.4 %all-gather.15.cloned.1.call-start = ((), (), s32[]{:S(2)}) async-start(), calls=%async_computation.5 | async-start | bytes 5242880 | tf_op jit(solution)/shard_map/all_gather | solution.py:119
  137.6 3.7 copy-start.3
  142.7 248.1 %all-gather.17.cloned.1.call-start = ((), (), s32[]{:S(2)}) async-start(), calls=%async_computation.6 | async-start | bytes 7208960 | tf_op jit(solution)/shard_map/all_gather | solution.py:124
  144.0 7.1 %copy-start.7 = (f32[1,1408]{1,0:T(1,128)S(1)}, f32[1,1408]{1,0:T(1,128)}, u32[]{:S(2)}) copy-start(f32[1,1408]{1,0:T(1,128)} %param.27) | copy-start | bytes 16900
  144.0 7.2 %copy-start.8 = (f32[1,1408]{1,0:T(1,128)S(1)}, f32[1,1408]{1,0:T(1,128)}, u32[]{:S(2)}) copy-start(f32[1,1408]{1,0:T(1,128)} %param.29) | copy-start | bytes 16900
  144.0 7.2 %copy-start.10 = (f32[1,512]{1,0:T(1,128)S(1)}, f32[1,512]{1,0:T(1,128)}, u32[]{:S(2)}) copy-start(f32[1,512]{1,0:T(1,128)} %param.33) | copy-start | bytes 6148
  144.0 46.7 %copy-start.5 = (f32[3,1408]{1,0:T(4,128)S(1)}, f32[3,1408]{1,0:T(4,128)}, u32[]{:S(2)}) copy-start(f32[3,1408]{1,0:T(4,128)} %param.31) | copy-start | bytes 50692
  144.0 46.7 %copy-start.6 = (f32[3,1408]{1,0:T(4,128)S(1)}, f32[3,1408]{1,0:T(4,128)}, u32[]{:S(2)}) copy-start(f32[3,1408]{1,0:T(4,128)} %param.30) | copy-start | bytes 50692
  144.0 356.2 %all-gather.19.cloned.1.call-start = ((), (), s32[]{:S(2)}) async-start(), calls=%async_computation.7 | async-start | bytes 7208960 | tf_op jit(solution)/shard_map/all_gather | solution.py:125
  147.3 436.7 %reduce-scatter.2.cloned.1.call-start = ((), (), s32[]{:S(2)}) async-start(), calls=%async_computation.8 | async-start | bytes 5242880 | tf_op jit(solution)/shard_map/reduce_scatter | solution.py:143
  149.7 241.1 %copy-start.14 = (f32[2048]{0:T(1024)S(1)}, f32[2048]{0:T(1024)}, u32[]{:S(2)}) copy-start(f32[2048]{0:T(1024)} %param.25) | copy-start | bytes 24580
  149.7 41.2 %collective-permute-start = (bf16[1408,512]{1,0:T(8,128)(2,1)S(1)}, bf16[1408,512]{1,0:T(8,128)(2,1)S(1)}, u32[]{:S(2)}, u32[]{:S(2)}) collective-permute-start(bf16[1408,512]{1,0:T(8,128)(2,1)S(1)} %convert_element_type.140), channel_id=1, source_target_pairs={{0,4},{4,0},{8,12},{12,8},{1,5},{5,1},{9,13},{13,9},{2,6},{6,2},{1... | collective-permute-start | bytes 4325384 | tf_op jit(solution)/shard_map/ppermute | solution.py:17
  192.9 319.2 %collective-permute-start.1 = (bf16[1408,1024]{1,0:T(8,128)(2,1)}, bf16[1408,1024]{1,0:T(8,128)(2,1)S(1)}, u32[]{:S(2)}, u32[]{:S(2)}) collective-permute-start(bf16[1408,1024]{1,0:T(8,128)(2,1)} %maximum_select_fusion.4), channel_id=1, source_target_pairs={{0,8},{4,12},{8,0},{12,4},{1,9},{5,13},{9,1},{13,5},{2,10},{6,14},... | collective-permute-start | bytes 8650760 | tf_op jit(solution)/shard_map/ppermute | solution.py:17
  513.7 70.3 %copy-start.2 = (bf16[1024,512]{1,0:T(8,128)(2,1)S(1)}, bf16[1024,512]{1,0:T(8,128)(2,1)}, u32[]{:S(2)}) copy-start(bf16[1024,512]{1,0:T(8,128)(2,1)} %fusion.20) | copy-start | bytes 3145732
  513.7 72.8 %copy-start.1 = (bf16[2,128,128]{2,1,0:T(8,128)(2,1)S(1)}, bf16[2,128,128]{2,1,0:T(8,128)(2,1)}, u32[]{:S(2)}) copy-start(bf16[2,128,128]{2,1,0:T(8,128)(2,1)} %param.21) | copy-start | bytes 196612
  (3 other events, 6.9 us)
Sparse Core Ops, SparseCore 0:
  8.9 37.1 all-gather.20
  47.7 27.9 all-gather.8
  77.3 27.3 all-gather.12
  106.1 31.4 all-gather.10
  142.8 32.9 all-gather.14
  177.2 213.5 all-gather.16
  392.4 107.8 all-gather.18
  541.4 42.5 reduce-scatter.1
